TPU v7x, 32 devices: a whole 2x2x4 slice. The times are simulated.
32 devices in a mesh: rep: 2 (over x), fs: 4 (over z), tp: 4 (over y, core).
Axes of the slice: x: 2, y: 2, z: 4, core: 2. Of those that a mesh axis runs over, the one named last changes fastest.
Arguments:
- tokens: bfloat16 [8192, 1024], P(('rep', 'fs', 'tp')), may hold values from -6 to 6
- norm_gain: float32 [1024], replicated, may hold values from 0.5 to 1.5
- gate_weight: bfloat16 [1024, 3072], P(('rep', 'fs'), 'tp'), may hold values from -0.1875 to 0.1875
- up_weight: bfloat16 [1024, 3072], P(('rep', 'fs'), 'tp'), may hold values from -0.1875 to 0.1875
- down_weight: bfloat16 [3072, 1024], P('tp', ('rep', 'fs')), may hold values from -0.109375 to 0.109375
Outputs:
- block_out: bfloat16 [8192, 1024], P(('rep', 'fs', 'tp'))
All inputs are finite; a program needn't handle non-finite values.
Results may differ from a plain program's by a relative error of at most 0.001.
Values may be sent and summed in bfloat16 or wider, within the bound.
A program may use at most 64 MiB of HBM per device.

v0:
```python
import jax
import jax.numpy as jnp
from jax import lax
from jax.sharding import PartitionSpec as P

epsilon = 1e-06


def over_all(shard, axis, dim, absorb, carry):
    whole = jax.tree.map(lambda part: lax.all_gather(part, axis, axis=dim, tiled=True), shard)
    return absorb(carry, whole, jnp.int32(0))


def summed_rows(portion, width, axis):
    count = width * lax.axis_size(axis)
    return lax.psum_scatter(portion(jnp.int32(0), count), axis, scatter_dimension=0, tiled=True)


def on_device(tokens, norm_gain, gate_weight, up_weight, down_weight):
    values = tokens.astype(jnp.float32)
    inverse_rms = lax.rsqrt(jnp.mean(values * values, axis=-1, keepdims=True) + epsilon)
    normed = (values * inverse_rms * norm_gain.astype(jnp.float32)).astype(jnp.bfloat16)
    gathered = lax.all_gather(normed, "tp", axis=0, tiled=True)
    zero_sums = jnp.zeros((gathered.shape[0], gate_weight.shape[1]), jnp.float32)

    def add_block(running, row_block, first_row):
        columns = lax.dynamic_slice_in_dim(gathered, first_row, row_block.shape[0], 1)
        return running + jnp.dot(columns, row_block, preferred_element_type=jnp.float32)

    gate_value = over_all(gate_weight, ("rep", "fs"), 0, add_block, zero_sums)
    up_value = over_all(up_weight, ("rep", "fs"), 0, add_block, zero_sums)
    hidden = (jax.nn.silu(gate_value) * up_value).astype(jnp.bfloat16)
    own_half = lax.all_gather(down_weight, "fs", axis=1, tiled=True)
    down_whole = lax.all_gather(own_half, "rep", axis=1, tiled=True)
    own_rows = tokens.shape[0]

    def row_terms(first_row, row_count):
        token_block = lax.dynamic_slice_in_dim(hidden, first_row, row_count, 0)
        return jnp.dot(token_block, down_whole, preferred_element_type=jnp.float32)

    mixed_out = summed_rows(row_terms, own_rows, "tp")
    return mixed_out.astype(jnp.bfloat16)


def solution(mesh):
    return jax.shard_map(
        on_device,
        mesh=mesh,
        in_specs=(
            P(("rep", "fs", "tp"), None),
            P(),
            P(("rep", "fs"), "tp"),
            P(("rep", "fs"), "tp"),
            P("tp", ("rep", "fs")),
        ),
        out_specs=P(("rep", "fs", "tp"), None),
        check_vma=False,
    )
```

profile of v0, /device:TPU:0, one launch (start us, length us, event | category | flops | bytes accessed | tf_op | source)
XLA Modules:
  0.0 218.2 jit_solution(9125715528160293608)
XLA Ops:
  6.5 0.0 all-gather.7.cloned.1.call-start
  6.5 0.7 all-gather.7.cloned.1.call-update
  7.3 0.0 all-gather.5.cloned.1.call-start
  7.3 1.2 fusion.1
  8.5 2.0 fusion.3
  10.6 0.0 all-gather.5.cloned.1.call-update
  10.6 0.0 all-gather.11.cloned.1.call-start
  10.6 0.0 copy-done
  10.7 27.4 %all_gather.18 = bf16[768,512]{1,0:T(8,128)(2,1)} all-gather(bf16[768,128]{1,0:T(8,128)(2,1)S(1)} %copy-done), channel_id=1, replica_groups=mesh['rep'=2,'fs'=4,'tp'=4] {'fs'}, dimensions={1}, use_global_device_ids=true | all-gather | bytes 983040 | tf_op jit(solution)/shard_map/all_gather | solution.py:33
  38.1 0.0 all-gather.11.cloned.1.call-update
  38.1 0.0 all-gather.9.cloned.1.call-start
  38.1 0.5 all-gather.9.cloned.1.call-update
  38.7 0.0 reduce-scatter.2.cloned.1.call-start
  38.7 20.9 %all-gather.7.cloned.1.call-done = bf16[1024,768]{1,0:T(8,128)(2,1)} async-done(((bf16[128,768]{1,0:T(8,128)(2,1)}), bf16[1024,768]{1,0:T(8,128)(2,1)}) %all-gather.7.cloned.1.call-update) | async-done | bytes 1572880 | tf_op jit(solution)/shard_map/all_gather | solution.py:10
  59.6 22.7 %all-gather.5.cloned.1.call-done = bf16[1024,1024]{1,0:T(8,128)(2,1)} async-done(((bf16[256,1024]{1,0:T(8,128)(2,1)}), bf16[1024,1024]{1,0:T(8,128)(2,1)}) %all-gather.5.cloned.1.call-update) | async-done | bytes 2097168 | tf_op jit(solution)/shard_map/all_gather | solution.py:23
  82.3 0.0 copy-start.1
  82.3 5.7 %fusion.5 = f32[1024,768]{1,0:T(8,128)} fusion(bf16[1024,1024]{1,0:T(8,128)(2,1)} %all-gather.5.cloned.1.call-done, bf16[1024,768]{1,0:T(8,128)(2,1)} %all-gather.7.cloned.1.call-done), kind=kOutput, calls=%fused_computation.9 | convolution fusion | flops 1610612736 | bytes 6815744 | tf_op jit(solution)/shard_map/dot_general | solution.py:28
  88.0 23.0 %all-gather.11.cloned.1.call-done = bf16[768,1024]{1,0:T(8,128)(2,1)} async-done(((bf16[768,512]{1,0:T(8,128)(2,1)}), bf16[768,1024]{1,0:T(8,128)(2,1)}) %all-gather.11.cloned.1.call-update) | async-done | bytes 1572880 | tf_op jit(solution)/shard_map/all_gather | solution.py:34
  111.0 46.1 %all-gather.9.cloned.1.call-done = bf16[1024,768]{1,0:T(8,128)(2,1)} async-done(((bf16[128,768]{1,0:T(8,128)(2,1)}), bf16[1024,768]{1,0:T(8,128)(2,1)}) %all-gather.9.cloned.1.call-update) | async-done | bytes 1572880 | tf_op jit(solution)/shard_map/all_gather | solution.py:10
  157.1 0.0 copy-done.1
  157.1 9.1 %fusion = f32[1024,1024]{1,0:T(8,128)} fusion(bf16[768,1024]{1,0:T(8,128)(2,1)} %all-gather.11.cloned.1.call-done, f32[1024,768]{1,0:T(8,128)} %fusion.5, bf16[1024,1024]{1,0:T(8,128)(2,1)S(1)} %copy-done.1, bf16[1024,768]{1,0:T(8,128)(2,1)} %all-gather.9.cloned.1.call-done), kind=kOutput, calls=%fused_computation.1 | convolution fusion | flops 3225944064 | bytes 12582912 | tf_op jit(solution)/shard_map/dot_general | solution.py:39
  166.3 0.0 reduce-scatter.2.cloned.1.call-update
  166.3 43.3 %reduce-scatter.2.cloned.1.call-done = f32[256,1024]{1,0:T(8,128)} async-done(((f32[1024,1024]{1,0:T(8,128)}), f32[256,1024]{1,0:T(8,128)}) %reduce-scatter.2.cloned.1.call-update) | async-done | bytes 1048592 | tf_op jit(solution)/shard_map/reduce_scatter | solution.py:16
  209.6 2.1 convert_element_type.15
  (2 shorter events, 0.0 us)
Async XLA Ops:
  6.5 4.1 %copy-start = (bf16[768,128]{1,0:T(8,128)(2,1)S(1)}, bf16[768,128]{1,0:T(8,128)(2,1)}, u32[]{:S(2)}) copy-start(bf16[768,128]{1,0:T(8,128)(2,1)} %param.9) | copy-start | bytes 589828
  6.5 53.1 %all-gather.7.cloned.1.call-start = ((), (), s32[]{:S(2)}) async-start(), calls=%async_computation.2 | async-start | bytes 1769472 | tf_op jit(solution)/shard_map/all_gather | solution.py:10
  7.3 75.1 %all-gather.5.cloned.1.call-start = ((), (), s32[]{:S(2)}) async-start(), calls=%async_computation.1 | async-start | bytes 2621440 | tf_op jit(solution)/shard_map/all_gather | solution.py:23
  10.6 100.4 %all-gather.11.cloned.1.call-start = ((), (), s32[]{:S(2)}) async-start(), calls=%async_computation.4 | async-start | bytes 2359296 | tf_op jit(solution)/shard_map/all_gather | solution.py:34
  38.1 119.0 %all-gather.9.cloned.1.call-start = ((), (), s32[]{:S(2)}) async-start(), calls=%async_computation.3 | async-start | bytes 1769472 | tf_op jit(solution)/shard_map/all_gather | solution.py:10
  38.7 170.9 %reduce-scatter.2.cloned.1.call-start = ((), (), s32[]{:S(2)}) async-start(), calls=%async_computation.5 | async-start | bytes 5242880 | tf_op jit(solution)/shard_map/reduce_scatter | solution.py:16
  82.3 74.8 %copy-start.1 = (bf16[1024,1024]{1,0:T(8,128)(2,1)S(1)}, bf16[1024,1024]{1,0:T(8,128)(2,1)}, u32[]{:S(2)}) copy-start(bf16[1024,1024]{1,0:T(8,128)(2,1)} %all-gather.5.cloned.1.call-done) | copy-start | bytes 6291460
Sparse Core Ops, SparseCore 0:
  9.4 50.1 all-gather.6
  61.2 21.0 all-gather.4
  83.9 27.0 all-gather.10
  112.9 44.1 all-gather.8
  166.4 43.1 reduce-scatter.1
where the time goes:
time: 218 us
  waiting for transfers between devices  157 us (72%)
  blocking collectives  27.4 us (13%)
  matrix products  14.8 us (7%)
  between operations  13.2 us (6%)
  other arithmetic  5.36 us (2%)
    all_gather x2, waiting for transfers between devices, over_all(): lax.all_gather(part, axis, axis=dim, tiled=True)  67.1 us
    reduce_scatter x1, waiting for transfers between devices, summed_rows(): lax.psum_scatter(portion(jnp.int32(0), count), axis, scatter_dimension=0,...  43.3 us
    all_gather x1, blocking collectives, on_device(): own_half = lax.all_gather(down_weight, 'fs', axis=1, tiled=True)  27.4 us
    all_gather x1, waiting for transfers between devices, on_device(): down_whole = lax.all_gather(own_half, 'rep', axis=1, tiled=True)  23 us
    all_gather x1, waiting for transfers between devices, on_device(): gathered = lax.all_gather(normed, 'tp', axis=0, tiled=True)  22.7 us
    dot_general x1, matrix products, row_terms(): return jnp.dot(token_block, down_whole, preferred_element_type=jnp.float32)  9.14 us
    dot_general x1, matrix products, add_block(): jnp.dot(columns, row_block, preferred_element_type=jnp.float32)  5.65 us
  transfers between devices with their start and end apart: 5, of which 5 were waited for; matrix products, arithmetic and copies ran while one was open for 4% of the time, Pallas kernels for 0%

commit v1 on v0

--- a/solution.py
+++ b/solution.py
@@ -1,9 +1,14 @@
+import functools
+
 import jax
 import jax.numpy as jnp
 from jax import lax
+from jax.experimental import pallas as pl
+from jax.experimental.pallas import tpu as pltpu
 from jax.sharding import PartitionSpec as P
 
 epsilon = 1e-06
+MESH = pl.DeviceIdType.MESH
 
 
 def over_all(shard, axis, dim, absorb, carry):
@@ -42,9 +47,243 @@
     return mixed_out.astype(jnp.bfloat16)
 
 
+def kernel(
+    fs_size, tok_ref, gain_ref, g_ref, u_ref, d_ref, out_ref,
+    gbuf, ubuf, dbuf, tokbuf, xn, gacc, uacc, hid, psend, precv, pkeep,
+    ring_send, ring_recv, pair_send, pair_recv, peer_send, peer_recv, tok_sem,
+):
+    n = 2 * fs_size
+    half = n // 2
+    rows, width = tok_ref.shape
+    depth, cols = g_ref.shape
+    out_cols = d_ref.shape[1]
+    tile = 256
+
+    rep, fs, tp = lax.axis_index("rep"), lax.axis_index("fs"), lax.axis_index("tp")
+    place = fs + rep * (n - 1 - 2 * fs)
+
+    def at_place(q):
+        rep_q = q // fs_size
+        return rep_q, q + rep_q * (n - 1 - 2 * q)
+
+    def device_at(q):
+        rep_q, fs_q = at_place(q)
+        return {"rep": rep_q, "fs": fs_q, "tp": tp}
+
+    def block_of(slot):
+        rep_q, fs_q = at_place((place + n - slot) % n)
+        return rep_q * fs_size + fs_q
+
+    right, left = device_at((place + 1) % n), device_at((place + n - 1) % n)
+    partner = {"rep": rep, "fs": fs, "tp": tp + 1 - 2 * (tp % 2)}
+    peer = {"rep": rep, "fs": fs, "tp": (tp + 2) % 4}
+
+    own, buf = (g_ref, u_ref, d_ref), (gbuf, ubuf, dbuf)
+
+    def held(kind, side, slot):
+        return own[kind] if side == 0 and slot == 0 else buf[kind].at[side, slot]
+
+    def ring(kind, way, slot):
+        to = slot + 1 if way == 0 else (slot - 1) % n
+        src, dst = held(kind, 0, slot), buf[kind].at[0, to]
+        if kind == 2 and to == half:
+            part = pl.ds(way * (cols // 2), cols // 2)
+            src, dst = src.at[part], dst.at[part]
+        return pltpu.make_async_remote_copy(
+            src_ref=src, dst_ref=dst,
+            send_sem=ring_send.at[way, kind, slot], recv_sem=ring_recv.at[way, kind, to],
+            device_id=right if way == 0 else left, device_id_type=MESH,
+        )
+
+    def pair(kind, slot):
+        return pltpu.make_async_remote_copy(
+            src_ref=held(kind, 0, slot), dst_ref=buf[kind].at[1, slot],
+            send_sem=pair_send.at[kind, slot], recv_sem=pair_recv.at[kind, slot],
+            device_id=partner, device_id_type=MESH,
+        )
+
+    def out_copy(slot):
+        return pltpu.make_async_remote_copy(
+            src_ref=psend.at[slot], dst_ref=precv.at[slot],
+            send_sem=peer_send.at[slot], recv_sem=peer_recv.at[slot],
+            device_id=peer, device_id_type=MESH,
+        )
+
+    tok_copy = pltpu.make_async_remote_copy(
+        src_ref=tok_ref, dst_ref=tokbuf, send_sem=tok_sem.at[0], recv_sem=tok_sem.at[1],
+        device_id=peer, device_id_type=MESH,
+    )
+    sent = []
+
+    def start(copy):
+        copy.start()
+        sent.append(copy)
+
+    barrier = pltpu.get_barrier_semaphore()
+    for device in (left, right, partner, peer):
+        pl.semaphore_signal(barrier, inc=1, device_id=device, device_id_type=MESH)
+    pl.semaphore_wait(barrier, 4)
+
+    for kind in (0, 1):
+        for way in (0, 1):
+            start(ring(kind, way, 0))
+    start(tok_copy)
+    for kind in (0, 1, 2):
+        start(pair(kind, 0))
+
+    def arrive(kind, k):
+        for way in (0, 1):
+            last = kind < 2 and k == half - 1 and way != kind
+            slot = k if way == 0 else n - k
+            ring(kind, way, (slot - 1) if way == 0 else (slot + 1) % n).wait_recv()
+            if not last:
+                start(ring(kind, way, slot))
+            start(pair(kind, slot))
+
+    def normalize(ref, first):
+        step = 32
+
+        @pl.loop(0, rows // step)
+        def _(i):
+            values = ref[pl.ds(pl.multiple_of(i * step, step), step), :].astype(jnp.float32)
+            scale = lax.rsqrt(jnp.mean(values * values, axis=-1, keepdims=True) + epsilon)
+            normed = (values * scale * gain_ref[...]).astype(jnp.bfloat16)
+            where = pl.ds(pl.multiple_of(first + i * step, step), step)
+            for b in range(n):
+                xn[b, where, :] = normed[:, b * depth:(b + 1) * depth]
+
+    def project(kind, k):
+        acc = (gacc, uacc)[kind]
+        a, b = (k, n - k) if k else (0, half)
+        lhs_a, lhs_b = block_of(a), block_of(b)
+        for side in (0, 1):
+            for slot in (a, b):
+                if side == 1:
+                    pair(kind, slot).wait_recv()
+
+            @pl.loop(0, cols // tile)
+            def _(i):
+                cut = pl.ds(pl.multiple_of(i * tile, tile), tile)
+                lhs = jnp.concatenate([xn[lhs_a], xn[lhs_b]], axis=1)
+                rhs = jnp.concatenate([held(kind, side, a)[:, cut], held(kind, side, b)[:, cut]], axis=0)
+                part = jnp.dot(lhs, rhs, preferred_element_type=jnp.float32)
+                to = pl.ds(pl.multiple_of(side * cols + i * tile, tile), tile)
+                if k == 1:
+                    acc[:, to] = part
+                else:
+                    acc[:, to] += part
+
+    def down(slots):
+        for slot in slots:
+            pair(2, slot).wait_recv()
+        rhs = jnp.concatenate(
+            [jnp.concatenate([held(2, side, slot)[...] for side in (0, 1)], axis=0) for slot in slots], axis=1
+        )
+        for first, store in ((0, psend), (rows, pkeep)):
+            part = jnp.dot(hid[first:first + rows, :], rhs, preferred_element_type=jnp.float32)
+            for j, slot in enumerate(slots):
+                store[slot] = part[:, j * out_cols:(j + 1) * out_cols]
+        for slot in slots:
+            start(out_copy(slot))
+
+    normalize(tok_ref, rows)
+    arrive(0, 1)
+    arrive(1, 1)
+    tok_copy.wait_recv()
+    normalize(tokbuf, 0)
+    project(0, 1)
+    for k in range(2, half):
+        arrive(0, k)
+        project(1, k - 1)
+        arrive(1, k)
+        project(0, k)
+    start(ring(2, 0, 0))
+    start(ring(2, 1, 0))
+    project(1, half - 1)
+    ring(0, 0, half - 1).wait_recv()
+    start(pair(0, half))
+    ring(1, 1, half + 1).wait_recv()
+    start(pair(1, half))
+    project(0, 0)
+    project(1, 0)
+
+    @pl.loop(0, 2 * rows // 16)
+    def _(i):
+        where = pl.ds(pl.multiple_of(i * 16, 16), 16)
+        gate = gacc[where, :]
+        hid[where, :] = (gate / (1.0 + jnp.exp(-gate)) * uacc[where, :]).astype(jnp.bfloat16)
+
+    down((0,))
+    for k in range(1, half):
+        arrive(2, k)
+        down((k, n - k))
+    ring(2, 0, half - 1).wait_recv()
+    ring(2, 1, half + 1).wait_recv()
+    start(pair(2, half))
+    down((half,))
+
+    order = [0] + [s for k in range(1, half) for s in (k, n - k)] + [half]
+    for slot in order:
+        out_copy(slot).wait_recv()
+        to = pl.ds(pl.multiple_of(block_of(slot) * out_cols, out_cols), out_cols)
+        out_ref[:, to] = (pkeep[slot] + precv[slot]).astype(out_ref.dtype)
+    for copy in sent:
+        copy.wait_send()
+
+
+def fused(fs_size, tokens, norm_gain, gate_weight, up_weight, down_weight):
+    n = 2 * fs_size
+    rows, width = tokens.shape
+    depth, cols = gate_weight.shape
+    out_cols = down_weight.shape[1]
+    vmem = pl.BlockSpec(memory_space=pltpu.VMEM)
+    bf16, f32 = jnp.bfloat16, jnp.float32
+    dma = pltpu.SemaphoreType.DMA
+    return pl.pallas_call(
+        functools.partial(kernel, fs_size),
+        out_shape=jax.ShapeDtypeStruct((rows, width), bf16),
+        in_specs=[vmem] * 5,
+        out_specs=vmem,
+        scratch_shapes=[
+            pltpu.VMEM((2, n, depth, cols), bf16),
+            pltpu.VMEM((2, n, depth, cols), bf16),
+            pltpu.VMEM((2, n, cols, out_cols), bf16),
+            pltpu.VMEM((rows, width), bf16),
+            pltpu.VMEM((n, 2 * rows, depth), bf16),
+            pltpu.VMEM((2 * rows, 2 * cols), f32),
+            pltpu.VMEM((2 * rows, 2 * cols), f32),
+            pltpu.VMEM((2 * rows, 2 * cols), bf16),
+            pltpu.VMEM((n, rows, out_cols), f32),
+            pltpu.VMEM((n, rows, out_cols), f32),
+            pltpu.VMEM((n, rows, out_cols), f32),
+            dma((2, 3, n)),
+            dma((2, 3, n)),
+            dma((3, n)),
+            dma((3, n)),
+            dma((n,)),
+            dma((n,)),
+            dma((2,)),
+        ],
+        compiler_params=pltpu.CompilerParams(
+            collective_id=0, has_side_effects=True, vmem_limit_bytes=60 * 1024 * 1024
+        ),
+    )(tokens, norm_gain.astype(f32).reshape(1, width), gate_weight, up_weight, down_weight)
+
+
 def solution(mesh):
+    sizes = dict(mesh.shape)
+
+    def run(tokens, norm_gain, gate_weight, up_weight, down_weight):
+        covered = (
+            sizes["rep"] == 2 and sizes["tp"] == 4 and sizes["fs"] >= 2
+            and gate_weight.shape[0] % 128 == 0 and gate_weight.shape[1] % 256 == 0
+            and down_weight.shape[1] % 128 == 0 and tokens.shape[0] % 32 == 0
+        )
+        body = functools.partial(fused, sizes["fs"]) if covered else on_device
+        return body(tokens, norm_gain, gate_weight, up_weight, down_weight)
+
     return jax.shard_map(
-        on_device,
+        run,
         mesh=mesh,
         in_specs=(
             P(("rep", "fs", "tp"), None),

time: 218 us -> 71.7 us (0.33)
  waiting for transfers between devices: 157 us -> 0 us
  Pallas kernels: 0 us -> 69.6 us
  blocking collectives: 27.4 us -> 0 us
  matrix products: 14.8 us -> 0 us
  between operations: 13.2 us -> 0.01 us
  other arithmetic: 5.36 us -> 0 us
    all_gather x4 -> x0, waiting for transfers between devices: 113 us -> none  [the longest x2 67.1 us: over_all(): lax.all_gather(part, axis, axis=dim, tiled=True)]
    pallas_call x0 -> x1, Pallas kernels: none -> 69.6 us  [fused(): pl.pallas_call(functools.partial(kernel, fs_size), out_shape=jax.ShapeDty...]
    reduce_scatter x1 -> x0, waiting for transfers between devices: 43.3 us -> none  [summed_rows(): lax.psum_scatter(portion(jnp.int32(0), count), axis, scatter_dimension=0,...]
    all_gather x1 -> x0, blocking collectives: 27.4 us -> none  [on_device(): own_half = lax.all_gather(down_weight, 'fs', axis=1, tiled=True)]
    dot_general x2 -> x0, matrix products: 14.8 us -> none  [the longest x1 9.14 us: row_terms(): return jnp.dot(token_block, down_whole, preferred_element_type=jnp.float32)]
    convert_element_type x2 -> x0, other arithmetic: 4.13 us -> none  [the longest x1 2.09 us: on_device(): return mixed_out.astype(jnp.bfloat16)]
  transfers between devices with their start and end apart: 5 -> 0, of which waited for: 5 -> 0; matrix products, arithmetic and copies ran while one was open for 4% -> 0% of each run, Pallas kernels for 0% -> 0%
where the time goes in v1:
time: 71.7 us; the launch traced here: 71.5 us
  Pallas kernels  69.6 us (97%)
  local copies, waits for them, and re-layouts  1.87 us (3%)
    pallas_call x1, Pallas kernels, fused(): pl.pallas_call(functools.partial(kernel, fs_size), out_shape=jax.ShapeDty...  69.6 us
    unnamed x1, local copies, waits for them, and re-layouts  1.87 us

profile of v1, /device:TPU:0, one launch (start us, length us, event | category | flops | bytes accessed | tf_op | source)
XLA Modules:
  0.0 71.5 jit_solution(16955769897734921351)
XLA Ops:
  0.0 69.6 %shard_map.55 = bf16[256,1024]{1,0:T(8,128)(2,1)} custom-call(bf16[256,1024]{1,0:T(8,128)(2,1)} %tok_ref.1, f32[1,1024]{1,0:T(1,128)} %bitcast.1, bf16[128,768]{1,0:T(8,128)(2,1)} %g_ref.1, bf16[128,768]{1,0:T(8,128)(2,1)} %u_ref.1, bf16[768,128]{1,0:T(8,128)(2,1)} %d_ref.1), custom_call_target="tpu_custom_call" | custom-call | tf_op jit(solution)/shard_map/pallas_call | solution.py:242
  69.6 1.9 %copy.7 = bf16[256,1024]{1,0:T(8,128)(2,1)} copy(bf16[256,1024]{1,0:T(8,128)(2,1)} %shard_map.55) | data formatting | bytes 1048576
